TPU v7x, 32 devices: a whole 2x2x4 slice. The times are simulated.
32 devices in a mesh: sp: 16 (over z, y, x), tp: 2 (over core).
Axes of the slice: x: 2, y: 2, z: 4, core: 2. Of those that a mesh axis runs over, the one named last changes fastest.
Arguments:
- queries: bfloat16 [8192, 2048], P('sp', 'tp'), may hold values from -14 to 14
- key_states: bfloat16 [8192, 512], P('sp', 'tp'), may hold values from -14 to 14
- value_states: bfloat16 [8192, 512], P('sp', 'tp'), may hold values from -6 to 6
- sink_logits: float32 [32], P('tp'), may hold values from 0 to 5
- out_weight: bfloat16 [2048, 2048], P('tp'), may hold values from -0.125 to 0.125
- residual: bfloat16 [8192, 2048], P(('sp', 'tp')), may hold values from -6 to 6
- gain_attn: float32 [2048], replicated, may hold values from 0.1 to 1.9
- gain_before: float32 [2048], replicated, may hold values from 0.1 to 1.9
- gain_after: float32 [2048], replicated, may hold values from 0.1 to 1.9
- gate_weight: bfloat16 [2048, 5632], P('sp', 'tp'), may hold values from -0.125 to 0.125
- value_weight: bfloat16 [2048, 5632], P('sp', 'tp'), may hold values from -0.125 to 0.125
- gate_taps: float32 [3, 5632], P(None, 'tp'), may hold values from -3 to 3
- value_taps: float32 [3, 5632], P(None, 'tp'), may hold values from -3 to 3
- down_weight: bfloat16 [5632, 2048], P('tp', 'sp'), may hold values from -0.078125 to 0.078125
Outputs:
- layer_out: bfloat16 [8192, 2048], P(('sp', 'tp'))
All inputs are finite; a program needn't handle non-finite values.
Results may differ from a plain program's by a relative error of at most 0.018.
Values may be sent and summed in bfloat16 or wider, within the bound.
A program may use at most 128 MiB of HBM per device.

v0:
```python
import jax
import jax.numpy as jnp
from jax import lax
from jax.sharding import PartitionSpec as P

HD = 64
WINDOW = 128


NEG_FILL = -1e30


def passed_along(block, axis, distance):
    devices = range(lax.axis_size(axis))
    route = [(i - distance, i) for i in devices if i - distance in devices]
    return lax.ppermute(block, axis, route)


def rms_scale(matrix):
    return matrix * lax.rsqrt(jnp.mean(matrix * matrix, axis=-1, keepdims=True) + 1e-06)


def attention_local(queries, key_states, value_states, sink_logits):
    length = queries.shape[0]
    blocks = length // WINDOW
    kv_local = key_states.shape[1] // HD
    grouping = queries.shape[1] // key_states.shape[1]
    earlier_keys, earlier_values = passed_along(
        (key_states[length - WINDOW :], value_states[length - WINDOW :]), "sp", 1
    )
    keys_ext = jnp.concatenate([earlier_keys, key_states], axis=0).reshape(
        blocks + 1, WINDOW, kv_local, HD
    )
    values_ext = jnp.concatenate([earlier_values, value_states], axis=0).reshape(
        blocks + 1, WINDOW, kv_local, HD
    )
    key_blocks = jnp.concatenate([keys_ext[:-1], keys_ext[1:]], axis=1)
    value_blocks = jnp.concatenate([values_ext[:-1], values_ext[1:]], axis=1)
    query_blocks = queries.reshape(blocks, WINDOW, kv_local, grouping, HD)
    offset = lax.axis_index("sp") * length
    qpos = (offset + jnp.arange(length, dtype=jnp.int32)).reshape(blocks, WINDOW)
    kpos = jnp.concatenate([qpos - WINDOW, qpos], axis=1)
    visible = (
        (kpos[:, None, :] <= qpos[:, :, None])
        & (qpos[:, :, None] - kpos[:, None, :] < WINDOW)
        & (kpos[:, None, :] >= 0)
    )
    scores = jnp.einsum(
        "nqhgd,nkhd->nhgqk", query_blocks, key_blocks, preferred_element_type=jnp.float32
    ) * HD ** (-0.5)
    scores = jnp.where(visible[:, None, None], scores, NEG_FILL)
    sink_col = sink_logits.reshape(kv_local, grouping)[None, :, :, None]
    top = jnp.maximum(jnp.max(scores, axis=-1), sink_col)
    expo = jnp.exp(scores - top[..., None])
    total = jnp.sum(expo, axis=-1) + jnp.exp(sink_col - top)
    probs = (expo / total[..., None]).astype(jnp.bfloat16)
    result = jnp.einsum(
        "nhgqk,nkhd->nqhgd", probs, value_blocks, preferred_element_type=jnp.float32
    )
    return result.astype(jnp.bfloat16).reshape(length, queries.shape[1])


def causal_local(upward, earlier, kernel):
    length = upward.shape[0]
    padded = jnp.concatenate([earlier, upward], axis=0).astype(jnp.float32)
    result = jnp.zeros(upward.shape, jnp.float32)
    for tap_index in range(kernel.shape[0]):
        result = result + kernel[tap_index][None, :] * padded[tap_index : tap_index + length]
    return result


def on_device(
    queries,
    key_states,
    value_states,
    sink_logits,
    out_weight,
    residual,
    gain_attn,
    gain_before,
    gain_after,
    gate_weight,
    value_weight,
    gate_taps,
    value_taps,
    down_weight,
):
    length = queries.shape[0]
    attended = attention_local(queries, key_states, value_states, sink_logits)
    selected = attended
    attn_proj = lax.psum_scatter(
        jnp.dot(selected, out_weight, preferred_element_type=jnp.float32).astype(jnp.bfloat16),
        "tp",
        scatter_dimension=0,
        tiled=True,
    ).astype(jnp.float32)
    middle = residual.astype(jnp.float32) + rms_scale(attn_proj) * gain_attn
    normed = (rms_scale(middle) * gain_before).astype(jnp.bfloat16)
    whole_rows = lax.all_gather(normed, "tp", axis=0, tiled=True)
    gate_full, value_full = (
        lax.all_gather(gate_weight, "sp", axis=0, tiled=True),
        lax.all_gather(value_weight, "sp", axis=0, tiled=True),
    )
    gate_up = jnp.dot(whole_rows, gate_full, preferred_element_type=jnp.float32).astype(
        jnp.bfloat16
    )
    value_up = jnp.dot(whole_rows, value_full, preferred_element_type=jnp.float32).astype(
        jnp.bfloat16
    )
    reach = gate_taps.shape[0] - 1
    gate_before, value_before = passed_along(
        (gate_up[length - reach :], value_up[length - reach :]), "sp", 1
    )
    gate_conv = causal_local(gate_up, gate_before, gate_taps)
    value_conv = causal_local(value_up, value_before, value_taps)
    hidden = (jax.nn.silu(gate_conv) * value_conv).astype(jnp.bfloat16)
    down_whole = lax.all_gather(down_weight, "sp", axis=1, tiled=True)
    selected = hidden
    down = lax.psum_scatter(
        jnp.dot(selected, down_whole, preferred_element_type=jnp.float32).astype(jnp.bfloat16),
        "tp",
        scatter_dimension=0,
        tiled=True,
    ).astype(jnp.float32)
    return (middle + rms_scale(down) * gain_after).astype(jnp.bfloat16)


def solution(mesh):
    in_specs = (
        P("sp", "tp"),
        P("sp", "tp"),
        P("sp", "tp"),
        P("tp"),
        P("tp", None),
        P(("sp", "tp"), None),
        P(),
        P(),
        P(),
        P("sp", "tp"),
        P("sp", "tp"),
        P(None, "tp"),
        P(None, "tp"),
        P("tp", "sp"),
    )
    out_specs = P(("sp", "tp"), None)
    return jax.shard_map(
        on_device, mesh=mesh, in_specs=in_specs, out_specs=out_specs, check_vma=False
    )
```

profile of v0, /device:TPU:0, one launch (start us, length us, event | category | flops | bytes accessed | tf_op | source)
XLA Modules:
  0.0 590.4 jit_solution(16810572428895233333)
XLA Ops:
  6.5 1.5 slice.72
  8.1 5.5 collective-permute-start.1
  13.6 1.5 slice.68
  15.0 3.4 collective-permute-start
  18.5 0.3 fusion.28
  18.8 1.2 reshape.89
  20.0 1.2 reshape.87
  21.3 4.3 reshape.90
  25.6 0.9 copy.24
  26.6 0.1 max.17
  26.6 1.0 copy.20
  27.6 0.9 pad_maximum_fusion
  28.5 0.2 reshape.88
  28.7 0.3 copy.23
  29.0 2.7 fusion.1
  31.8 3.1 copy-done
  34.9 2.4 fusion
  37.3 0.1 exponential_add_fusion
  37.4 0.9 pad_maximum_fusion.1
  38.3 0.2 reshape.86
  38.5 0.3 copy.19
  38.8 5.8 fusion.20
  44.5 0.9 copy.28
  45.5 3.7 convolution_convert_fusion.2
  49.3 0.3 all-gather.5.cloned.1.call-start
  49.5 9.3 %reduce-scatter.3.cloned.1.call-done = bf16[256,2048]{1,0:T(8,128)(2,1)} async-done(((bf16[512,2048]{1,0:T(8,128)(2,1)}), bf16[256,2048]{1,0:T(8,128)(2,1)}) %reduce-scatter.3.cloned.1.call-update) | async-done | bytes 1048592 | tf_op jit(solution)/shard_map/reduce_scatter | solution.py:91
  58.9 1.5 fusion.10
  60.4 1.8 multiply_reduce_fusion
  62.3 2.8 multiply_convert_fusion
  65.1 0.7 all-gather.7.cloned.1.call-update
  65.9 0.5 all-gather.9.cloned.1.call-update
  66.5 0.5 all-gather.11.cloned.1.call-update
  67.1 0.2 slice_reduce_fusion.2
  67.2 9.9 %all-gather.5.cloned.1.call-done = bf16[512,2048]{1,0:T(8,128)(2,1)} async-done(((bf16[256,2048]{1,0:T(8,128)(2,1)}), bf16[512,2048]{1,0:T(8,128)(2,1)}) %all-gather.5.cloned.1.call-update) | async-done | bytes 2097168 | tf_op jit(solution)/shard_map/all_gather | solution.py:99
  77.1 145.4 %all-gather.7.cloned.1.call-done = bf16[2048,2816]{1,0:T(8,128)(2,1)} async-done(((bf16[128,2816]{1,0:T(8,128)(2,1)}), bf16[2048,2816]{1,0:T(8,128)(2,1)}) %all-gather.7.cloned.1.call-update) | async-done | bytes 11534352 | tf_op jit(solution)/shard_map/all_gather | solution.py:101
  222.5 10.9 %convolution_convert_fusion.1 = bf16[512,2816]{1,0:T(8,128)(2,1)S(1)} fusion(bf16[512,2048]{1,0:T(8,128)(2,1)} %all-gather.5.cloned.1.call-done, bf16[2048,2816]{1,0:T(8,128)(2,1)} %all-gather.7.cloned.1.call-done), kind=kOutput, calls=%fused_computation.18 | convolution fusion | flops 5907021824 | bytes 16515072 | tf_op jit(solution)/shard_map/dot_general | solution.py:104
  233.4 1.6 copy-done.3
  235.1 3.2 collective-permute-start.2
  238.3 126.7 %all-gather.9.cloned.1.call-done = bf16[2048,2816]{1,0:T(8,128)(2,1)} async-done(((bf16[128,2816]{1,0:T(8,128)(2,1)}), bf16[2048,2816]{1,0:T(8,128)(2,1)}) %all-gather.9.cloned.1.call-update) | async-done | bytes 11534352 | tf_op jit(solution)/shard_map/all_gather | solution.py:102
  365.0 11.1 %convolution_convert_fusion = bf16[512,2816]{1,0:T(8,128)(2,1)S(1)} fusion(bf16[512,2048]{1,0:T(8,128)(2,1)} %all-gather.5.cloned.1.call-done, bf16[2048,2816]{1,0:T(8,128)(2,1)} %all-gather.9.cloned.1.call-done), kind=kOutput, calls=%fused_computation.17 | convolution fusion | flops 5907021824 | bytes 16515072 | tf_op jit(solution)/shard_map/dot_general | solution.py:107
  376.1 3.4 collective-permute-start.3
  379.5 3.1 maximum_convert_fusion
  382.6 3.1 maximum_convert_fusion.1
  385.7 162.1 %all-gather.11.cloned.1.call-done = bf16[2816,2048]{1,0:T(8,128)(2,1)} async-done(((bf16[2816,128]{1,0:T(8,128)(2,1)}), bf16[2816,2048]{1,0:T(8,128)(2,1)}) %all-gather.11.cloned.1.call-update) | async-done | bytes 11534352 | tf_op jit(solution)/shard_map/all_gather | solution.py:117
  547.8 23.2 %convolution_convert_fusion.3 = bf16[512,2048]{1,0:T(8,128)(2,1)} fusion(bf16[2816,2048]{1,0:T(8,128)(2,1)} %all-gather.11.cloned.1.call-done, f32[514,2816]{1,0:T(8,128)} %maximum_convert_fusion.1, f32[514,2816]{1,0:T(8,128)} %maximum_convert_fusion, f32[2816]{0:T(1024)S(1)} %get-tuple-element.9, f32[2816]{0:T(1024)S(1)} %get-tuple-element.10, ...), kind=kOutput, calls=%fused_computation.21 | convolution fusion | flops 5929697280 | bytes 48302080 | tf_op jit(solution)/shard_map/dot_general | solution.py:120
  571.0 8.1 %reduce-scatter.5.cloned.1.call-done = bf16[256,2048]{1,0:T(8,128)(2,1)} async-done(((bf16[512,2048]{1,0:T(8,128)(2,1)}), bf16[256,2048]{1,0:T(8,128)(2,1)}) %reduce-scatter.5.cloned.1.call-update) | async-done | bytes 1048592 | tf_op jit(solution)/shard_map/reduce_scatter | solution.py:119
  579.1 1.5 fusion.13
  580.6 2.9 fusion.16
  (50 shorter events, 0.4 us)
Async XLA Ops:
  6.5 21.1 %copy-start.5 = (bf16[512,256]{1,0:T(8,128)(2,1)S(1)}, bf16[512,256]{1,0:T(8,128)(2,1)}, u32[]{:S(2)}) copy-start(bf16[512,256]{1,0:T(8,128)(2,1)} %param.15) | copy-start | bytes 786436
  6.5 20.0 %copy-start.13 = (f32[16]{0:T(128)S(1)}, f32[16]{0:T(128)}, u32[]{:S(2)}) copy-start(f32[16]{0:T(128)} %param.17) | copy-start | bytes 196
  6.5 52.3 %reduce-scatter.3.cloned.1.call-start = ((), (), s32[]{:S(2)}) async-start(), calls=%async_computation.2 | async-start | bytes 3145728 | tf_op jit(solution)/shard_map/reduce_scatter | solution.py:91
  8.1 19.6 %collective-permute-start.1 = (bf16[128,256]{1,0:T(8,128)(2,1)}, bf16[128,256]{1,0:T(8,128)(2,1)}, u32[]{:S(2)}, u32[]{:S(2)}) collective-permute-start(bf16[128,256]{1,0:T(8,128)(2,1)} %slice.72), channel_id=1, source_target_pairs={{0,2},{2,4},{4,6},{6,8},{8,10},{10,12},{12,14},{14,16},{16,18},{18... | collective-permute-start | bytes 196616 | tf_op jit(solution)/shard_map/ppermute | solution.py:16
  15.0 22.4 %collective-permute-start = (bf16[128,256]{1,0:T(8,128)(2,1)}, bf16[128,256]{1,0:T(8,128)(2,1)}, u32[]{:S(2)}, u32[]{:S(2)}) collective-permute-start(bf16[128,256]{1,0:T(8,128)(2,1)} %slice.68), channel_id=1, source_target_pairs={{0,2},{2,4},{4,6},{6,8},{8,10},{10,12},{12,14},{14,16},{16,18},{18... | collective-permute-start | bytes 196616 | tf_op jit(solution)/shard_map/ppermute | solution.py:16
  31.7 3.2 copy-start
  31.7 5.7 copy-start.6
  31.7 7.1 %copy-start.7 = (bf16[4,128,4,64]{1,3,2,0:T(8,128)(2,1)S(1)}, bf16[4,128,4,64]{1,3,2,0:T(8,128)(2,1)}, u32[]{:S(2)}) copy-start(bf16[4,128,4,64]{1,3,2,0:T(8,128)(2,1)} %copy.20) | copy-start | bytes 786436
  38.8 6.7 %copy-start.14 = (bf16[1024,2048]{1,0:T(8,128)(2,1)S(1)}, bf16[1024,2048]{1,0:T(8,128)(2,1)}, u32[]{:S(2)}) copy-start(bf16[1024,2048]{1,0:T(8,128)(2,1)} %param.18) | copy-start | bytes 12582916
  45.5 14.9 %copy-start.2 = (bf16[256,2048]{1,0:T(8,128)(2,1)S(1)}, bf16[256,2048]{1,0:T(8,128)(2,1)}, u32[]{:S(2)}) copy-start(bf16[256,2048]{1,0:T(8,128)(2,1)} %param.19) | copy-start | bytes 3145732
  45.5 14.9 %copy-start.8 = (f32[2048]{0:T(1024)S(1)}, f32[2048]{0:T(1024)}, u32[]{:S(2)}) copy-start(f32[2048]{0:T(1024)} %param.20) | copy-start | bytes 24580
  45.5 16.8 %copy-start.11 = (f32[2048]{0:T(1024)S(1)}, f32[2048]{0:T(1024)}, u32[]{:S(2)}) copy-start(f32[2048]{0:T(1024)} %param.21) | copy-start | bytes 24580
  49.2 17.8 %copy-start.9 = (f32[3,2816]{1,0:T(4,128)S(1)}, f32[3,2816]{1,0:T(4,128)}, u32[]{:S(2)}) copy-start(f32[3,2816]{1,0:T(4,128)} %param.26) | copy-start | bytes 101380
  49.2 17.8 %copy-start.10 = (f32[3,2816]{1,0:T(4,128)S(1)}, f32[3,2816]{1,0:T(4,128)}, u32[]{:S(2)}) copy-start(f32[3,2816]{1,0:T(4,128)} %param.25) | copy-start | bytes 101380
  49.3 27.8 %all-gather.5.cloned.1.call-start = ((), (), s32[]{:S(2)}) async-start(), calls=%async_computation.3 | async-start | bytes 3145728 | tf_op jit(solution)/shard_map/all_gather | solution.py:99
  65.1 157.4 %all-gather.7.cloned.1.call-start = ((), (), s32[]{:S(2)}) async-start(), calls=%async_computation.4 | async-start | bytes 12255232 | tf_op jit(solution)/shard_map/all_gather | solution.py:101
  65.8 299.1 %all-gather.9.cloned.1.call-start = ((), (), s32[]{:S(2)}) async-start(), calls=%async_computation.5 | async-start | bytes 12255232 | tf_op jit(solution)/shard_map/all_gather | solution.py:102
  66.4 481.4 %all-gather.11.cloned.1.call-start = ((), (), s32[]{:S(2)}) async-start(), calls=%async_computation.6 | async-start | bytes 12255232 | tf_op jit(solution)/shard_map/all_gather | solution.py:117
  67.0 512.1 %reduce-scatter.5.cloned.1.call-start = ((), (), s32[]{:S(2)}) async-start(), calls=%async_computation.7 | async-start | bytes 3145728 | tf_op jit(solution)/shard_map/reduce_scatter | solution.py:119
  233.4 1.6 copy-start.3
  235.1 144.4 %collective-permute-start.2 = (bf16[2,2816]{1,0:T(2,128)(2,1)S(1)}, bf16[2,2816]{1,0:T(2,128)(2,1)S(1)}, u32[]{:S(2)}, u32[]{:S(2)}) collective-permute-start(bf16[2,2816]{1,0:T(2,128)(2,1)S(1)} %slice.90), channel_id=1, source_target_pairs={{0,2},{2,4},{4,6},{6,8},{8,10},{10,12},{12,14},{14,16},{16,18},{18... | collective-permute-start | bytes 33800 | tf_op jit(solution)/shard_map/ppermute | solution.py:16
  365.0 14.5 %copy-start.4 = (bf16[512,2816]{1,0:T(8,128)(2,1)S(1)}, bf16[512,2816]{1,0:T(8,128)(2,1)}, u32[]{:S(2)}) copy-start(bf16[512,2816]{1,0:T(8,128)(2,1)} %copy-done.3) | copy-start | bytes 8650756
  376.1 6.6 %collective-permute-start.3 = (bf16[2,2816]{1,0:T(2,128)(2,1)S(1)}, bf16[2,2816]{1,0:T(2,128)(2,1)S(1)}, u32[]{:S(2)}, u32[]{:S(2)}) collective-permute-start(bf16[2,2816]{1,0:T(2,128)(2,1)S(1)} %slice.94), channel_id=1, source_target_pairs={{0,2},{2,4},{4,6},{6,8},{8,10},{10,12},{12,14},{14,16},{16,18},{18... | collective-permute-start | bytes 33800 | tf_op jit(solution)/shard_map/ppermute | solution.py:16
  547.8 32.8 %copy-start.1 = (bf16[256,2048]{1,0:T(8,128)(2,1)S(1)}, bf16[256,2048]{1,0:T(8,128)(2,1)}, u32[]{:S(2)}) copy-start(bf16[256,2048]{1,0:T(8,128)(2,1)} %reduce-scatter.3.cloned.1.call-done) | copy-start | bytes 3145732
  547.8 32.8 %copy-start.12 = (f32[2048]{0:T(1024)S(1)}, f32[2048]{0:T(1024)}, u32[]{:S(2)}) copy-start(f32[2048]{0:T(1024)} %param.22) | copy-start | bytes 24580
Sparse Core Ops, SparseCore 0:
  49.4 9.4 reduce-scatter.2
  65.2 11.8 all-gather.4
  79.9 142.5 all-gather.6
  225.1 139.8 all-gather.8
  367.5 180.2 all-gather.10
  571.1 7.9 reduce-scatter.4
where the time goes:
time: 591 us; the launch traced here: 590 us
  waiting for transfers between devices  463 us (78%)
  matrix products  57.3 us (10%)
  other arithmetic  21.4 us (4%)
  local copies, waits for them, and re-layouts  18.7 us (3%)
  starting transfers between devices  15.9 us (3%)
  between operations  13.8 us (2%)
    all_gather x1, waiting for transfers between devices, on_device(): down_whole = lax.all_gather(down_weight, 'sp', axis=1, tiled=True)  162 us
    all_gather x1, waiting for transfers between devices, on_device(): lax.all_gather(gate_weight, 'sp', axis=0, tiled=True)  145 us
    all_gather x1, waiting for transfers between devices, on_device(): lax.all_gather(value_weight, 'sp', axis=0, tiled=True)  127 us
    dot_general x1, matrix products, on_device(): jnp.dot(selected, down_whole, preferred_element_type=jnp.float32)  23.2 us
    ppermute x4, starting transfers between devices, passed_along(): return lax.ppermute(block, axis, route)  15.5 us
  transfers between devices with their start and end apart: 10, of which 6 were waited for; matrix products, arithmetic and copies ran while one was open for 8% of the time, Pallas kernels for 0%

commit v1 on v0

--- a/solution.py
+++ b/solution.py
@@ -1,14 +1,20 @@
+import functools
+
 import jax
 import jax.numpy as jnp
 from jax import lax
+from jax.experimental import pallas as pl
+from jax.experimental.pallas import tpu as pltpu
 from jax.sharding import PartitionSpec as P
 
 HD = 64
 WINDOW = 128
+TEAM = 4
 
 
 NEG_FILL = -1e30
-
+MESH = pl.DeviceIdType.MESH
+VMEM_BYTES = 60 * 1024 * 1024
 
 def passed_along(block, axis, distance):
     devices = range(lax.axis_size(axis))
@@ -69,7 +75,7 @@
     return result
 
 
-def on_device(
+def on_device_plain(
     queries,
     key_states,
     value_states,
@@ -125,6 +131,467 @@
     return (middle + rms_scale(down) * gain_after).astype(jnp.bfloat16)
 
 
+def team_peer(place, turn):
+    low, high = place % 2, place // 2
+    if turn & 1:
+        low = 1 - low
+    if turn & 2:
+        high = 1 - high
+    return high * 2 + low
+
+
+def remote(src, dst, send, recv, **device):
+    return pltpu.make_async_remote_copy(
+        src_ref=src, dst_ref=dst, send_sem=send, recv_sem=recv, device_id=device, device_id_type=MESH
+    )
+
+
+def greet(devices):
+    barrier = pltpu.get_barrier_semaphore()
+    for device in devices:
+        pl.semaphore_signal(barrier, inc=1, device_id=device, device_id_type=MESH)
+    pl.semaphore_wait(barrier, len(devices))
+
+
+def row_scale(block):
+    return lax.rsqrt(jnp.mean(block * block, axis=-1, keepdims=True) + 1e-06)
+
+
+def front_kernel(
+    ring,
+    q_ref,
+    k_ref,
+    v_ref,
+    sink_ref,
+    ow_ref,
+    res_ref,
+    ga_ref,
+    gb_ref,
+    gate_in,
+    value_in,
+    down_in,
+    rows_all,
+    gate_all,
+    value_all,
+    down_all,
+    mid_ref,
+    k_ext,
+    v_ext,
+    att,
+    snd,
+    rcv,
+    own,
+    nrm,
+    halo_s,
+    halo_r,
+    trade_s,
+    trade_r,
+    local_sem,
+    ring_s,
+    ring_r,
+    pair_s,
+    pair_r,
+    rows_s,
+    rows_r,
+    mate_s,
+    mate_r,
+):
+    sp, tp = lax.axis_index("sp"), lax.axis_index("tp")
+    members = ring * TEAM
+    level, place = sp // TEAM, sp % TEAM
+    up = (level + 1) % ring * TEAM + place
+    down = (level + ring - 1) % ring * TEAM + place
+    after, before = (sp + 1) % members, (sp + members - 1) % members
+    mate = 1 - tp
+    length = q_ref.shape[0]
+    share = length // 2
+    deep = gate_in.shape[1]
+    units = gate_in.shape[2]
+    wide = down_in.shape[1]
+    sends = []
+
+    greet(
+        [{"sp": level * TEAM + team_peer(place, turn)} for turn in range(1, TEAM)]
+        + [{"tp": mate}, {"sp": up}, {"sp": down}, {"sp": after}, {"sp": before}]
+    )
+
+    def begin(copy):
+        copy.start()
+        sends.append(copy)
+        return copy
+
+    halos = [
+        begin(
+            remote(
+                ref.at[pl.ds(length - WINDOW, WINDOW)],
+                ext.at[pl.ds(0, WINDOW)],
+                halo_s.at[i],
+                halo_r.at[i],
+                sp=after,
+            )
+        )
+        for i, (ref, ext) in enumerate(((k_ref, k_ext), (v_ref, v_ext)))
+    ]
+
+    def span(m, ref, start, size):
+        if m < 2:
+            return ref.at[pl.ds(pl.multiple_of(start * deep, deep), size * deep)]
+        return ref.at[:, pl.ds(pl.multiple_of(start * wide, wide), size * wide)]
+
+    def piece(m, member):
+        if m < 2:
+            return (gate_in, value_in)[m].at[member]
+        return down_in.at[pl.ds(pl.multiple_of(member * units, units), units)]
+
+    wholes = (gate_all, value_all, down_all)
+    trades, locals_ = [], []
+    for m in range(3):
+        trades.append(
+            [
+                begin(
+                    remote(
+                        piece(m, team_peer(place, turn)),
+                        span(m, wholes[m], sp, 1),
+                        trade_s.at[m, turn - 1],
+                        trade_r.at[m, turn - 1],
+                        sp=level * TEAM + team_peer(place, turn),
+                    )
+                )
+                for turn in (3, 1, 2)
+            ]
+        )
+        copy = pltpu.make_async_copy(piece(m, place), span(m, wholes[m], sp, 1), local_sem.at[m])
+        copy.start()
+        locals_.append(copy)
+
+    last = ring // 2
+    ring_copies = {}
+
+    def ring_start(m, step):
+        if step == 1:
+            locals_[m].wait()
+            for copy in trades[m]:
+                copy.wait_recv()
+        for side, towards in ((0, up), (1, down)):
+            if step > 1:
+                ring_copies[m, step - 1, side].wait_recv()
+            source = (level + ring - (step - 1)) % ring if side == 0 else (level + step - 1) % ring
+            if step < last:
+                block = span(m, wholes[m], source * TEAM, TEAM)
+            else:
+                block = span(m, wholes[m], source * TEAM + side * (TEAM // 2), TEAM // 2)
+            sems = (ring_s.at[m, step - 1, side], ring_r.at[m, step - 1, side])
+            ring_copies[m, step, side] = begin(remote(block, block, *sems, sp=towards))
+
+    k_ext[pl.ds(WINDOW, length)] = k_ref[...]
+    v_ext[pl.ds(WINDOW, length)] = v_ref[...]
+    for copy in halos:
+        copy.wait_recv()
+    heads_kv = k_ref.shape[1] // HD
+    grouping = q_ref.shape[1] // k_ref.shape[1]
+    row = lax.broadcasted_iota(jnp.int32, (WINDOW, 2 * WINDOW), 0)
+    col = lax.broadcasted_iota(jnp.int32, (WINDOW, 2 * WINDOW), 1)
+    band = (col <= row + WINDOW) & (col > row)
+
+    for kv in range(heads_kv):
+
+        def block_step(n, carry, kv=kv):
+            start = pl.multiple_of(n * WINDOW, WINDOW)
+            keys = k_ext[pl.ds(start, 2 * WINDOW), kv * HD : (kv + 1) * HD]
+            values = v_ext[pl.ds(start, 2 * WINDOW), kv * HD : (kv + 1) * HD]
+            wide_q = q_ref[pl.ds(start, WINDOW), kv * grouping * HD : (kv + 1) * grouping * HD]
+            visible = band & (col + (sp * length + start - WINDOW) >= 0)
+            stacked = jnp.concatenate(
+                [wide_q[:, g * HD : (g + 1) * HD] for g in range(grouping)], axis=0
+            )
+            scores = lax.dot_general(
+                stacked, keys, (((1,), (1,)), ((), ())), preferred_element_type=jnp.float32
+            ) * HD ** (-0.5)
+            probs = []
+            for g in range(grouping):
+                sink = sink_ref[kv * grouping + g]
+                part = jnp.where(visible, scores[g * WINDOW : (g + 1) * WINDOW], NEG_FILL)
+                top = jnp.maximum(jnp.max(part, axis=-1, keepdims=True), sink)
+                expo = jnp.exp(part - top)
+                total = jnp.sum(expo, axis=-1, keepdims=True) + jnp.exp(sink - top)
+                probs.append((expo / total).astype(jnp.bfloat16))
+            result = jnp.dot(
+                jnp.concatenate(probs, axis=0), values, preferred_element_type=jnp.float32
+            ).astype(jnp.bfloat16)
+            att[pl.ds(start, WINDOW), kv * grouping * HD : (kv + 1) * grouping * HD] = (
+                jnp.concatenate(
+                    [result[g * WINDOW : (g + 1) * WINDOW] for g in range(grouping)], axis=1
+                )
+            )
+            return carry
+
+        lax.fori_loop(0, length // WINDOW, block_step, 0)
+        if kv < 3:
+            ring_start(kv, 1)
+    for m in range(min(heads_kv, 3), 3):
+        ring_start(m, 1)
+
+    columns = ow_ref.shape[1]
+    tile = min(512, columns)
+
+    def project(rows_start, target):
+        def tile_step(t, carry):
+            at = pl.multiple_of(t * tile, tile)
+            target[:, pl.ds(at, tile)] = jnp.dot(
+                att[pl.ds(rows_start, share)],
+                ow_ref[:, pl.ds(at, tile)],
+                preferred_element_type=jnp.float32,
+            ).astype(jnp.bfloat16)
+            return carry
+
+        lax.fori_loop(0, columns // tile, tile_step, 0)
+
+    project(pl.multiple_of(mate * share, share), snd)
+    pair = begin(remote(snd, rcv, pair_s, pair_r, tp=mate))
+    project(pl.multiple_of(tp * share, share), own)
+    pair.wait_recv()
+    band_rows = 32
+
+    def norm_step(t, carry):
+        at = pl.ds(pl.multiple_of(t * band_rows, band_rows), band_rows)
+        proj = own[at].astype(jnp.float32) + rcv[at].astype(jnp.float32)
+        middle = res_ref[at].astype(jnp.float32) + proj * row_scale(proj) * ga_ref[...]
+        mid_ref[at] = middle
+        nrm[at] = (middle * row_scale(middle) * gb_ref[...]).astype(jnp.bfloat16)
+        return carry
+
+    lax.fori_loop(0, share // band_rows, norm_step, 0)
+
+    def slot(member, core):
+        return rows_all.at[pl.ds(pl.multiple_of((member * 2 + core) * share, share), share)]
+
+    mates = [begin(remote(nrm, slot(place, tp), mate_s.at[0], mate_r.at[0], tp=mate))]
+    spread = {
+        turn: begin(
+            remote(
+                nrm,
+                slot(place, tp),
+                rows_s.at[turn - 1],
+                rows_r.at[turn - 1],
+                sp=level * TEAM + team_peer(place, turn),
+            )
+        )
+        for turn in (3, 1, 2)
+    }
+    mine = pltpu.make_async_copy(nrm, slot(place, tp), local_sem.at[3])
+    mine.start()
+    for step in range(2, last + 1):
+        for m in range(3):
+            ring_start(m, step)
+    for turn in (1, 2, 3):
+        spread[turn].wait_recv()
+        block = slot(team_peer(place, turn), tp)
+        mates.append(begin(remote(block, block, mate_s.at[turn], mate_r.at[turn], tp=mate)))
+    mine.wait()
+    for copy in mates:
+        copy.wait_recv()
+    for m in range(3):
+        for side in range(2):
+            ring_copies[m, last, side].wait_recv()
+    for copy in sends:
+        copy.wait_send()
+
+
+def back_kernel(
+    hid_ref, down_ref, mid_ref, gain_ref, out_ref, psnd, prcv, own, snd, rcv, ps, pr, ts, tr
+):
+    sp, tp = lax.axis_index("sp"), lax.axis_index("tp")
+    level, place = sp // TEAM, sp % TEAM
+    mate = 1 - tp
+    share = mid_ref.shape[0]
+    columns = down_ref.shape[1]
+    tile = min(512, columns)
+    greet(
+        [{"sp": level * TEAM + team_peer(place, turn)} for turn in range(1, TEAM)]
+        + [{"tp": mate}]
+    )
+    order = (3, 1, 2, 0)
+
+    def product(turn, core, store):
+        start = pl.multiple_of((team_peer(place, turn) * 2 + core) * share, share)
+
+        def tile_step(t, carry):
+            at = pl.ds(pl.multiple_of(t * tile, tile), tile)
+            part = jnp.dot(
+                hid_ref[pl.ds(start, share)], down_ref[:, at], preferred_element_type=jnp.float32
+            )
+            store(at, part)
+            return carry
+
+        lax.fori_loop(0, columns // tile, tile_step, 0)
+
+    pairs, sends = [], []
+    for i, turn in enumerate(order):
+
+        def to_mate(at, part, i=i):
+            psnd[i, :, at] = part.astype(jnp.bfloat16)
+
+        product(turn, mate, to_mate)
+        copy = remote(psnd.at[i], prcv.at[i], ps.at[i], pr.at[i], tp=mate)
+        copy.start()
+        pairs.append(copy)
+    for i, turn in enumerate(order):
+        pairs[i].wait_recv()
+
+        def add_mate(at, part, i=i, turn=turn):
+            total = part.astype(jnp.bfloat16).astype(jnp.float32) + prcv[i, :, at].astype(jnp.float32)
+            if turn:
+                snd[i, :, at] = total.astype(jnp.bfloat16)
+            else:
+                own[:, at] = total
+
+        product(turn, tp, add_mate)
+        if turn:
+            copy = remote(
+                snd.at[i],
+                rcv.at[i],
+                ts.at[i],
+                tr.at[i],
+                sp=level * TEAM + team_peer(place, turn),
+            )
+            copy.start()
+            sends.append(copy)
+    for copy in sends:
+        copy.wait_recv()
+    band_rows = 32
+
+    def norm_step(t, carry):
+        at = pl.ds(pl.multiple_of(t * band_rows, band_rows), band_rows)
+        total = own[at]
+        for i in range(TEAM - 1):
+            total = total + rcv[i, at].astype(jnp.float32)
+        out_ref[at] = (mid_ref[at] + total * row_scale(total) * gain_ref[...]).astype(out_ref.dtype)
+        return carry
+
+    lax.fori_loop(0, share // band_rows, norm_step, 0)
+    for copy in pairs + sends:
+        copy.wait_send()
+
+
+def on_device_team(
+    ring,
+    queries,
+    key_states,
+    value_states,
+    sink_logits,
+    out_weight,
+    residual,
+    gain_attn,
+    gain_before,
+    gain_after,
+    gate_weight,
+    value_weight,
+    gate_taps,
+    value_taps,
+    down_weight,
+):
+    length, width = queries.shape[0], residual.shape[1]
+    share = residual.shape[0]
+    deep, local_units = gate_weight.shape
+    units = local_units // TEAM
+    rows = length * TEAM
+    vmem = pl.BlockSpec(memory_space=pltpu.VMEM)
+    smem = pl.BlockSpec(memory_space=pltpu.SMEM)
+    far = pl.BlockSpec(memory_space=pl.ANY)
+    dma = pltpu.SemaphoreType.DMA
+    bf16, f32 = jnp.bfloat16, jnp.float32
+
+    def by_member(weight):
+        return weight.reshape(deep, TEAM, units).transpose(1, 0, 2)
+
+    steps = ring // 2
+    rows_all, gate_all, value_all, down_all, middle = pl.pallas_call(
+        functools.partial(front_kernel, ring),
+        out_shape=(
+            jax.ShapeDtypeStruct((rows, width), bf16),
+            jax.ShapeDtypeStruct((width, units), bf16),
+            jax.ShapeDtypeStruct((width, units), bf16),
+            jax.ShapeDtypeStruct((units, width), bf16),
+            jax.ShapeDtypeStruct((share, width), f32),
+        ),
+        in_specs=[vmem] * 3 + [smem] + [vmem] * 7,
+        out_specs=(far, far, far, far, vmem),
+        scratch_shapes=[
+            pltpu.VMEM((length + WINDOW, key_states.shape[1]), bf16),
+            pltpu.VMEM((length + WINDOW, key_states.shape[1]), bf16),
+            pltpu.VMEM(queries.shape, bf16),
+            pltpu.VMEM((share, width), bf16),
+            pltpu.VMEM((share, width), bf16),
+            pltpu.VMEM((share, width), bf16),
+            pltpu.VMEM((share, width), bf16),
+            dma((2,)),
+            dma((2,)),
+            dma((3, TEAM - 1)),
+            dma((3, TEAM - 1)),
+            dma((4,)),
+            dma((3, steps, 2)),
+            dma((3, steps, 2)),
+            dma(()),
+            dma(()),
+            dma((TEAM - 1,)),
+            dma((TEAM - 1,)),
+            dma((TEAM,)),
+            dma((TEAM,)),
+        ],
+        compiler_params=pltpu.CompilerParams(
+            collective_id=0, has_side_effects=True, vmem_limit_bytes=VMEM_BYTES
+        ),
+        name="front",
+    )(
+        queries,
+        key_states,
+        value_states,
+        sink_logits,
+        out_weight,
+        residual,
+        gain_attn[None],
+        gain_before[None],
+        by_member(gate_weight),
+        by_member(value_weight),
+        down_weight,
+    )
+    gate_up = jnp.dot(rows_all, gate_all, preferred_element_type=f32).astype(bf16)
+    value_up = jnp.dot(rows_all, value_all, preferred_element_type=f32).astype(bf16)
+    reach = gate_taps.shape[0] - 1
+    tails = passed_along(
+        jnp.concatenate([gate_up[rows - reach :], value_up[rows - reach :]], axis=0), "sp", TEAM
+    )
+    first = lax.axis_index("sp") % TEAM * units
+    gate_conv = causal_local(
+        gate_up, tails[:reach], lax.dynamic_slice_in_dim(gate_taps, first, units, 1)
+    )
+    value_conv = causal_local(
+        value_up, tails[reach:], lax.dynamic_slice_in_dim(value_taps, first, units, 1)
+    )
+    hidden = (jax.nn.silu(gate_conv) * value_conv).astype(bf16)
+    return pl.pallas_call(
+        back_kernel,
+        out_shape=jax.ShapeDtypeStruct((share, width), bf16),
+        in_specs=[vmem] * 4,
+        out_specs=vmem,
+        scratch_shapes=[
+            pltpu.VMEM((TEAM, share, width), bf16),
+            pltpu.VMEM((TEAM, share, width), bf16),
+            pltpu.VMEM((share, width), f32),
+            pltpu.VMEM((TEAM - 1, share, width), bf16),
+            pltpu.VMEM((TEAM - 1, share, width), bf16),
+            dma((TEAM,)),
+            dma((TEAM,)),
+            dma((TEAM - 1,)),
+            dma((TEAM - 1,)),
+        ],
+        compiler_params=pltpu.CompilerParams(
+            collective_id=1, has_side_effects=True, vmem_limit_bytes=VMEM_BYTES
+        ),
+        name="back",
+    )(hidden, down_all, middle, gain_after[None])
+
+
 def solution(mesh):
     in_specs = (
         P("sp", "tp"),
@@ -143,6 +610,16 @@
         P("tp", "sp"),
     )
     out_specs = P(("sp", "tp"), None)
+    members, cores = mesh.shape["sp"], mesh.shape["tp"]
+    ring = members // TEAM
+
+    def on_device(*args):
+        units, wide = args[13].shape
+        teams = cores == 2 and members % TEAM == 0 and ring >= 4 and ring % 2 == 0
+        if teams and units % (TEAM * 16) == 0 and wide % 128 == 0:
+            return on_device_team(ring, *args)
+        return on_device_plain(*args)
+
     return jax.shard_map(
         on_device, mesh=mesh, in_specs=in_specs, out_specs=out_specs, check_vma=False
     )

time: 591 us -> 275 us (0.47)
  waiting for transfers between devices: 463 us -> 0.17 us
  Pallas kernels: 0 us -> 233 us
  matrix products: 57.3 us -> 17 us
  between operations: 13.8 us -> 0.13 us
  starting transfers between devices: 15.9 us -> 3.65 us
  other arithmetic: 21.4 us -> 9.27 us
  local copies, waits for them, and re-layouts: 18.7 us -> 10.2 us
    all_gather x4 -> x0, waiting for transfers between devices: 444 us -> none  [the longest x1 162 us: on_device(): down_whole = lax.all_gather(down_weight, 'sp', axis=1, tiled=True)]
    pallas_call x0 -> x2, Pallas kernels: none -> 233 us  [the longest x1 171 us: on_device_team(): pl.pallas_call(functools.partial(front_kernel, ring), out_shape=(jax.Shap...]
    dot_general x6 -> x2, matrix products: 57.3 us -> 17 us  [the longest x1 10.2 us: on_device_team(): jnp.dot(rows_all, gate_all, preferred_element_type=f32).astype(bf16)]
    reduce_scatter x2 -> x0, waiting for transfers between devices: 17.4 us -> none  [the longest x1 9.34 us: on_device(): lax.psum_scatter(jnp.dot(selected, out_weight, preferred_element_type=jnp...]
    ppermute x4 -> x1, starting transfers between devices: 15.5 us -> 3.65 us  [passed_along(): return lax.ppermute(block, axis, route)]
    slice x12 -> x3, local copies, waits for them, and re-layouts: 8.41 us -> 0.02 us  [the longest x1 0.01 us: on_device_team(): tails[:reach]]
    reduce_sum x4 -> x0, other arithmetic: 7.24 us -> none  [the longest x3 4.86 us: rms_scale(): jnp.mean(matrix * matrix, axis=-1, keepdims=True) + 1e-06]
  transfers between devices with their start and end apart: 10 -> 1, of which waited for: 6 -> 1; matrix products, arithmetic and copies ran while one was open for 8% -> 0% of each run, Pallas kernels for 0% -> 0%
where the time goes in v1:
time: 275 us; the launch traced here: 274 us
  Pallas kernels  233 us (85%)
  matrix products  17 us (6%)
  local copies, waits for them, and re-layouts  10.2 us (4%)
  other arithmetic  9.27 us (3%)
  starting transfers between devices  3.65 us (1%)
    pallas_call x1, Pallas kernels, on_device_team(): pl.pallas_call(functools.partial(front_kernel, ring), out_shape=(jax.Shap...  171 us
    pallas_call x1, Pallas kernels, on_device_team(): pl.pallas_call(back_kernel, out_shape=jax.ShapeDtypeStruct((share, width)...  61.9 us
    dot_general x1, matrix products, on_device_team(): jnp.dot(rows_all, gate_all, preferred_element_type=f32).astype(bf16)  10.2 us
    unnamed x9, local copies, waits for them, and re-layouts  6.88 us
    dot_general x1, matrix products, on_device_team(): jnp.dot(rows_all, value_all, preferred_element_type=f32).astype(bf16)  6.87 us
    convert_element_type x1, other arithmetic, on_device_team(): hidden = (jax.nn.silu(gate_conv) * value_conv).astype(bf16)  6.16 us
  transfers between devices with their start and end apart: 1, of which 1 were waited for; matrix products, arithmetic and copies ran while one was open for 0% of the time, Pallas kernels for 0%

profile of v1, /device:TPU:0, one launch (start us, length us, event | category | flops | bytes accessed | tf_op | source)
XLA Modules:
  0.0 273.8 jit_solution(10836592200408868013)
XLA Ops:
  0.0 1.5 copy.17
  1.5 1.2 copy.18
  2.6 1.5 copy.19
  4.1 1.2 copy.20
  5.2 171.5 %front.1 = (bf16[2048,2048]{1,0:T(8,128)(2,1)}, bf16[2048,704]{1,0:T(8,128)(2,1)}, bf16[2048,704]{1,0:T(8,128)(2,1)}, bf16[704,2048]{1,0:T(8,128)(2,1)}, f32[256,2048]{1,0:T(8,128)}) custom-call(bf16[512,1024]{1,0:T(8,128)(2,1)} %q_ref.1, bf16[512,256]{1,0:T(8,128)(2,1)} %k_ref.1, bf16[512,256]{1,0:T(8,128)(2,1)} %v_ref.1, f32[16]{0:T(128)} %sink_ref.1, ...), custom_call_target="tpu_custom_call" | custom-call | tf_op jit(solution)/shard_map/front/pallas_call | solution.py:508
  176.7 0.0 copy-start.1
  176.7 0.0 copy-start.2
  176.7 10.2 %convolution_convert_fusion.1 = bf16[2048,704]{1,0:T(8,128)(2,1)S(1)} fusion(bf16[2048,2048]{1,0:T(8,128)(2,1)} %get-tuple-element.10, bf16[2048,704]{1,0:T(8,128)(2,1)} %get-tuple-element.11), kind=kOutput, calls=%fused_computation.13 | convolution fusion | flops 5907021824 | bytes 14155776 | tf_op jit(solution)/shard_map/dot_general | solution.py:558
  186.9 0.0 copy-done.1
  186.9 0.0 copy-done.2
  186.9 6.9 %convolution_convert_fusion = bf16[2048,704]{1,0:T(8,128)(2,1)S(1)} fusion(bf16[2048,2048]{1,0:T(8,128)(2,1)S(1)} %copy-done.1, bf16[2048,704]{1,0:T(8,128)(2,1)S(1)} %copy-done.2), kind=kOutput, calls=%fused_computation.12 | convolution fusion | flops 5907021824 | bytes 14155776 | tf_op jit(solution)/shard_map/dot_general | solution.py:559
  193.8 0.0 copy-start
  193.8 1.7 copy-done
  195.5 3.6 %collective-permute-start = (bf16[4,704]{1,0:T(4,128)(2,1)S(1)}, bf16[4,704]{1,0:T(4,128)(2,1)S(1)}, u32[]{:S(2)}, u32[]{:S(2)}) collective-permute-start(bf16[4,704]{1,0:T(4,128)(2,1)S(1)} %pad_maximum_fusion), channel_id=1, source_target_pairs={{0,8},{2,10},{4,12},{6,14},{8,16},{10,18},{12,20},{14,22},{16,24},... | collective-permute-start | bytes 16904 | tf_op jit(solution)/shard_map/ppermute | solution.py:22
  199.2 1.0 dynamic-slice_reduce_fusion.2
  200.1 0.2 collective-permute-done
  200.3 3.1 %maximum_convert_fusion = (f32[2050,704]{1,0:T(8,128)S(1)}, f32[2050,704]{1,0:T(8,128)S(1)}) fusion(bf16[2048,704]{1,0:T(8,128)(2,1)S(1)} %convolution_convert_fusion.1, bf16[2,704]{1,0:T(2,128)(2,1)S(1)} %get-tuple-element.21, bf16[2048,704]{1,0:T(8,128)(2,1)} %copy-done, bf16[2,704]{1,0:T(2,128)(2,1)S(1)} %get-tuple-element.22), kind=kLoop, calls=%fused_computation.14 | loop fusion | flops 11545600 | bytes 17318400 | tf_op jit(solution)/shard_map/convert_element_type | solution.py:71
  203.4 6.2 %fusion.2.hid_ref = bf16[2048,704]{1,0:T(8,128)(2,1)} fusion(f32[2050,704]{1,0:T(8,128)S(1)} %get-tuple-element.24, f32[2050,704]{1,0:T(8,128)S(1)} %get-tuple-element.23, f32[704]{0:T(1024)S(1)} %get-tuple-element.20, f32[704]{0:T(1024)S(1)} %get-tuple-element.19, f32[704]{0:T(1024)S(1)} %get-tuple-element.18, f32[704]{0:T(1024)S(1)} %get-tuple-element.25, ...), kind=kLoop, calls=%fused_computation.3 | loop fusion | flops 23068672 | bytes 37503488 | tf_op jit(solution)/shard_map/convert_element_type | solution.py:571
  209.6 61.9 %back.1 = bf16[256,2048]{1,0:T(8,128)(2,1)} custom-call(bf16[2048,704]{1,0:T(8,128)(2,1)} %fusion.2.hid_ref, bf16[704,2048]{1,0:T(8,128)(2,1)} %get-tuple-element.13.down_ref, f32[256,2048]{1,0:T(8,128)} %get-tuple-element.14.mid_ref, f32[1,2048]{1,0:T(1,128)} %bitcast.17), custom_call_target="tpu_custom_call" | custom-call | tf_op jit(solution)/shard_map/back/pallas_call | solution.py:572
  271.5 2.3 copy.26
  (4 shorter events, 0.0 us)
Async XLA Ops:
  176.7 10.2 %copy-start.1 = (bf16[2048,2048]{1,0:T(8,128)(2,1)S(1)}, bf16[2048,2048]{1,0:T(8,128)(2,1)}, u32[]{:S(2)}) copy-start(bf16[2048,2048]{1,0:T(8,128)(2,1)} %get-tuple-element.10) | copy-start | bytes 25165828
  176.7 10.2 %copy-start.2 = (bf16[2048,704]{1,0:T(8,128)(2,1)S(1)}, bf16[2048,704]{1,0:T(8,128)(2,1)}, u32[]{:S(2)}) copy-start(bf16[2048,704]{1,0:T(8,128)(2,1)} %get-tuple-element.12) | copy-start | bytes 8650756
  193.8 1.7 copy-start
  195.5 4.8 %collective-permute-start = (bf16[4,704]{1,0:T(4,128)(2,1)S(1)}, bf16[4,704]{1,0:T(4,128)(2,1)S(1)}, u32[]{:S(2)}, u32[]{:S(2)}) collective-permute-start(bf16[4,704]{1,0:T(4,128)(2,1)S(1)} %pad_maximum_fusion), channel_id=1, source_target_pairs={{0,8},{2,10},{4,12},{6,14},{8,16},{10,18},{12,20},{14,22},{16,24},... | collective-permute-start | bytes 16904 | tf_op jit(solution)/shard_map/ppermute | solution.py:22

commit v2 on v1

--- a/solution.py
+++ b/solution.py
@@ -170,11 +170,16 @@
     gate_in,
     value_in,
     down_in,
+    gate_taps,
+    value_taps,
+    hid_ref,
+    down_all,
+    mid_ref,
     rows_all,
     gate_all,
     value_all,
-    down_all,
-    mid_ref,
+    gate_up,
+    value_up,
     k_ext,
     v_ext,
     att,
@@ -195,6 +200,8 @@
     rows_r,
     mate_s,
     mate_r,
+    tail_s,
+    tail_r,
 ):
     sp, tp = lax.axis_index("sp"), lax.axis_index("tp")
     members = ring * TEAM
@@ -326,9 +333,9 @@
             return carry
 
         lax.fori_loop(0, length // WINDOW, block_step, 0)
-        if kv < 3:
+        if kv < 2:
             ring_start(kv, 1)
-    for m in range(min(heads_kv, 3), 3):
+    for m in range(min(heads_kv, 2), 2):
         ring_start(m, 1)
 
     columns = ow_ref.shape[1]
@@ -381,8 +388,9 @@
     mine = pltpu.make_async_copy(nrm, slot(place, tp), local_sem.at[3])
     mine.start()
     for step in range(2, last + 1):
-        for m in range(3):
+        for m in range(2):
             ring_start(m, step)
+    ring_start(2, 1)
     for turn in (1, 2, 3):
         spread[turn].wait_recv()
         block = slot(team_peer(place, turn), tp)
@@ -390,9 +398,62 @@
     mine.wait()
     for copy in mates:
         copy.wait_recv()
-    for m in range(3):
+
+    rows = rows_all.shape[0]
+    edge = gate_up.shape[0] - rows
+    tails = []
+    for m, result in enumerate((gate_up, value_up)):
         for side in range(2):
             ring_copies[m, last, side].wait_recv()
+
+        def up_step(t, carry, m=m, result=result):
+            at = pl.multiple_of(t * share, share)
+            result[pl.ds(pl.multiple_of(at + edge, edge), share)] = jnp.dot(
+                rows_all[pl.ds(at, share)], wholes[m][...], preferred_element_type=jnp.float32
+            ).astype(jnp.bfloat16)
+            return carry
+
+        lax.fori_loop(0, rows // share, up_step, 0)
+        tails.append(
+            begin(
+                remote(
+                    result.at[pl.ds(rows, edge)],
+                    result.at[pl.ds(0, edge)],
+                    tail_s.at[m],
+                    tail_r.at[m],
+                    sp=up,
+                )
+            )
+        )
+    for step in range(2, last + 1):
+        ring_start(2, step)
+    for tail, result in zip(tails, (gate_up, value_up)):
+        tail.wait_recv()
+        result[pl.ds(0, edge)] = jnp.where(
+            level > 0, result[pl.ds(0, edge)].astype(jnp.float32), 0.0
+        ).astype(jnp.bfloat16)
+    reach = gate_taps.shape[0] - 1
+    conv_rows = 64
+
+    def conv_step(t, carry):
+        at = pl.multiple_of(t * conv_rows, conv_rows)
+
+        def mixed(source, taps):
+            padded = source[pl.ds(at, conv_rows + edge)].astype(jnp.float32)
+            total = jnp.zeros((conv_rows, units), jnp.float32)
+            for k in range(reach + 1):
+                first = edge - reach + k
+                total = total + taps[k : k + 1, :] * padded[first : first + conv_rows]
+            return total
+
+        gate = mixed(gate_up, gate_taps)
+        value = mixed(value_up, value_taps)
+        hid_ref[pl.ds(at, conv_rows)] = (gate / (1.0 + jnp.exp(-gate)) * value).astype(jnp.bfloat16)
+        return carry
+
+    lax.fori_loop(0, rows // conv_rows, conv_step, 0)
+    for side in range(2):
+        ring_copies[2, last, side].wait_recv()
     for copy in sends:
         copy.wait_send()
 
@@ -505,18 +566,22 @@
         return weight.reshape(deep, TEAM, units).transpose(1, 0, 2)
 
     steps = ring // 2
-    rows_all, gate_all, value_all, down_all, middle = pl.pallas_call(
+    first = lax.axis_index("sp") % TEAM * units
+    hidden, down_all, middle = pl.pallas_call(
         functools.partial(front_kernel, ring),
         out_shape=(
-            jax.ShapeDtypeStruct((rows, width), bf16),
-            jax.ShapeDtypeStruct((width, units), bf16),
-            jax.ShapeDtypeStruct((width, units), bf16),
+            jax.ShapeDtypeStruct((rows, units), bf16),
             jax.ShapeDtypeStruct((units, width), bf16),
             jax.ShapeDtypeStruct((share, width), f32),
         ),
-        in_specs=[vmem] * 3 + [smem] + [vmem] * 7,
-        out_specs=(far, far, far, far, vmem),
+        in_specs=[vmem] * 3 + [smem] + [vmem] * 9,
+        out_specs=(vmem, far, vmem),
         scratch_shapes=[
+            pltpu.VMEM((rows, width), bf16),
+            pltpu.VMEM((width, units), bf16),
+            pltpu.VMEM((width, units), bf16),
+            pltpu.VMEM((rows + 16, units), bf16),
+            pltpu.VMEM((rows + 16, units), bf16),
             pltpu.VMEM((length + WINDOW, key_states.shape[1]), bf16),
             pltpu.VMEM((length + WINDOW, key_states.shape[1]), bf16),
             pltpu.VMEM(queries.shape, bf16),
@@ -537,6 +602,8 @@
             dma((TEAM - 1,)),
             dma((TEAM,)),
             dma((TEAM,)),
+            dma((2,)),
+            dma((2,)),
         ],
         compiler_params=pltpu.CompilerParams(
             collective_id=0, has_side_effects=True, vmem_limit_bytes=VMEM_BYTES
@@ -554,21 +621,9 @@
         by_member(gate_weight),
         by_member(value_weight),
         down_weight,
-    )
-    gate_up = jnp.dot(rows_all, gate_all, preferred_element_type=f32).astype(bf16)
-    value_up = jnp.dot(rows_all, value_all, preferred_element_type=f32).astype(bf16)
-    reach = gate_taps.shape[0] - 1
-    tails = passed_along(
-        jnp.concatenate([gate_up[rows - reach :], value_up[rows - reach :]], axis=0), "sp", TEAM
-    )
-    first = lax.axis_index("sp") % TEAM * units
-    gate_conv = causal_local(
-        gate_up, tails[:reach], lax.dynamic_slice_in_dim(gate_taps, first, units, 1)
-    )
-    value_conv = causal_local(
-        value_up, tails[reach:], lax.dynamic_slice_in_dim(value_taps, first, units, 1)
-    )
-    hidden = (jax.nn.silu(gate_conv) * value_conv).astype(bf16)
+        lax.dynamic_slice_in_dim(gate_taps, first, units, 1),
+        lax.dynamic_slice_in_dim(value_taps, first, units, 1),
+    )
     return pl.pallas_call(
         back_kernel,
         out_shape=jax.ShapeDtypeStruct((share, width), bf16),

time: 275 us -> 246 us (0.89)
  matrix products: 17 us -> 0 us
  other arithmetic: 9.27 us -> 0 us
  Pallas kernels: 233 us -> 237 us
  starting transfers between devices: 3.65 us -> 0 us
    dot_general x2 -> x0, matrix products: 17 us -> none  [the longest x1 10.2 us: on_device_team(): jnp.dot(rows_all, gate_all, preferred_element_type=f32).astype(bf16)]
    convert_element_type x2 -> x0, other arithmetic: 9.25 us -> none  [the longest x1 6.16 us: on_device_team(): hidden = (jax.nn.silu(gate_conv) * value_conv).astype(bf16)]
    ppermute x1 -> x0, starting transfers between devices: 3.65 us -> none  [passed_along(): return lax.ppermute(block, axis, route)]
    unnamed x9 -> x5, local copies, waits for them, and re-layouts: 6.88 us -> 4.11 us
  transfers between devices with their start and end apart: 1 -> 0, of which waited for: 1 -> 0; matrix products, arithmetic and copies ran while one was open for 0% -> 0% of each run, Pallas kernels for 0% -> 0%
where the time goes in v2:
time: 246 us; the launch traced here: 245 us
  Pallas kernels  237 us (96%)
  local copies, waits for them, and re-layouts  8.01 us (3%)
    pallas_call x1, Pallas kernels, on_device_team(): pl.pallas_call(functools.partial(front_kernel, ring), out_shape=(jax.Shap...  174 us
    pallas_call x1, Pallas kernels, on_device_team(): pl.pallas_call(back_kernel, out_shape=jax.ShapeDtypeStruct((share, width)...  63.3 us

profile of v2, /device:TPU:0, one launch (start us, length us, event | category | flops | bytes accessed | tf_op | source)
XLA Modules:
  0.0 245.4 jit_solution(10585238750922157842)
XLA Ops:
  0.0 0.0 copy-start
  0.0 1.5 constant_dynamic-slice_fusion
  1.5 1.5 copy.15
  2.9 1.2 copy.16
  4.1 0.0 copy-done
  4.1 0.3 copy.17
  4.5 1.2 copy.18
  5.7 174.0 %front.1 = (bf16[2048,704]{1,0:T(8,128)(2,1)}, bf16[704,2048]{1,0:T(8,128)(2,1)}, f32[256,2048]{1,0:T(8,128)}) custom-call(bf16[512,1024]{1,0:T(8,128)(2,1)} %q_ref.1, bf16[512,256]{1,0:T(8,128)(2,1)} %k_ref.1, bf16[512,256]{1,0:T(8,128)(2,1)} %v_ref.1, f32[16]{0:T(128)} %sink_ref.1, bf16[1024,2048]{1,0:T(8,128)(2,1)} %ow_ref.1, bf16[256,2048]{1,0:T(8,128)(2,1)} %res_ref.1, ...), custom_call_target="tpu_custom_call" | custom-call | tf_op jit(solution)/shard_map/front/pallas_call | solution.py:570
  179.7 63.3 %back.1 = bf16[256,2048]{1,0:T(8,128)(2,1)} custom-call(bf16[2048,704]{1,0:T(8,128)(2,1)} %get-tuple-element.8.hid_ref, bf16[704,2048]{1,0:T(8,128)(2,1)} %get-tuple-element.9.down_ref, f32[256,2048]{1,0:T(8,128)} %get-tuple-element.10.mid_ref, f32[1,2048]{1,0:T(1,128)} %bitcast.13), custom_call_target="tpu_custom_call" | custom-call | tf_op jit(solution)/shard_map/back/pallas_call | solution.py:627
  243.1 2.3 copy.20
Async XLA Ops:
  0.0 4.1 %copy-start = (bf16[128,2816]{1,0:T(8,128)(2,1)S(1)}, bf16[128,2816]{1,0:T(8,128)(2,1)}, u32[]{:S(2)}) copy-start(bf16[128,2816]{1,0:T(8,128)(2,1)} %param.24) | copy-start | bytes 2162692
